TPU v7x, 32 devices: a whole 2x2x4 slice. The times are simulated.
32 devices in a mesh: fs: 8 (over z, y), tp: 4 (over x, core).
Axes of the slice: x: 2, y: 2, z: 4, core: 2. Of those that a mesh axis runs over, the one named last changes fastest.
Arguments:
- saved_input: bfloat16 [6144, 2048], P('fs'), may hold values from -6 to 6
- cot_inproj: bfloat16 [6144, 1024], P('fs', 'tp'), may hold values from -0.076171875 to 0.076171875
- cot_outproj: bfloat16 [6144, 1024], P('fs', 'tp'), may hold values from -0.076171875 to 0.076171875
- factor_inproj: bfloat16 [2048, 256], P('fs')
- factor_outproj: bfloat16 [2048, 256], P('fs')
- weight_inproj: float32 [2048, 1024], P('fs', 'tp'), may hold values from -0.125 to 0.125
- weight_outproj: float32 [2048, 1024], P('fs', 'tp'), may hold values from -0.125 to 0.125
- first_inproj: float32 [256, 1024], P('fs', 'tp'), may hold values from -6 to 6
- first_outproj: float32 [256, 1024], P('fs', 'tp'), may hold values from -6 to 6
- second_inproj: float32 [256, 1024], P('fs', 'tp'), may hold values from 0.25 to 4
- second_outproj: float32 [256, 1024], P('fs', 'tp'), may hold values from 0.25 to 4
Outputs:
- update_inproj: float32 [2048, 1024], P('fs', 'tp')
- update_outproj: float32 [2048, 1024], P('fs', 'tp')
- new_inproj: float32 [2048, 1024], P('fs', 'tp')
- new_outproj: float32 [2048, 1024], P('fs', 'tp')
- copy_inproj: bfloat16 [2048, 1024], P(None, 'tp')
- copy_outproj: bfloat16 [2048, 1024], P(None, 'tp')
- first_inproj_new: float32 [256, 1024], P('fs', 'tp')
- first_outproj_new: float32 [256, 1024], P('fs', 'tp')
- second_inproj_new: float32 [256, 1024], P('fs', 'tp')
- second_outproj_new: float32 [256, 1024], P('fs', 'tp')
All inputs are finite; a program needn't handle non-finite values.
Results may differ from a plain program's by a relative error of at most 0.00045.
Values may be sent and summed in bfloat16 or wider, within the bound.
A program may use at most 64 MiB of HBM per device.

v0:
```python
import jax
import jax.numpy as jnp
from jax import lax
from jax.sharding import PartitionSpec as P


def contract_rows(left, right, precision):
    return lax.dot_general(
        left,
        right,
        (((0,), (0,)), ((), ())),
        precision=precision,
        preferred_element_type=jnp.float32,
    )


def on_device(
    saved_input,
    cot_inproj,
    cot_outproj,
    factor_inproj,
    factor_outproj,
    weight_inproj,
    weight_outproj,
    first_inproj,
    first_outproj,
    second_inproj,
    second_outproj,
):
    highest = lax.Precision.HIGHEST
    pieces = (
        lax.all_gather(factor_inproj, "fs", axis=0, tiled=True),
        lax.all_gather(factor_outproj, "fs", axis=0, tiled=True),
    )
    mapped_in = jnp.dot(saved_input, pieces[0], preferred_element_type=jnp.float32)
    mapped_out = jnp.dot(saved_input, pieces[1], preferred_element_type=jnp.float32)
    term_in = contract_rows(mapped_in, cot_inproj.astype(jnp.float32), highest)
    term_out = contract_rows(mapped_out, cot_outproj.astype(jnp.float32), highest)
    projected_in, projected_out = (
        lax.psum_scatter(term_in, "fs", scatter_dimension=0, tiled=True),
        lax.psum_scatter(term_out, "fs", scatter_dimension=0, tiled=True),
    )
    first_in_new = 0.8 * first_inproj + 0.2 * projected_in
    first_out_new = 0.8 * first_outproj + 0.2 * projected_out
    second_in_new = 0.9 * second_inproj + 0.1 * projected_in * projected_in
    second_out_new = 0.9 * second_outproj + 0.1 * projected_out * projected_out
    small_in = first_in_new / (jnp.sqrt(second_in_new) + 1e-08)
    small_out = first_out_new / (jnp.sqrt(second_out_new) + 1e-08)
    wide_in = factor_inproj.astype(jnp.float32)
    wide_out = factor_outproj.astype(jnp.float32)
    pieces = (
        lax.all_gather(small_in, "fs", axis=0, tiled=True),
        lax.all_gather(small_out, "fs", axis=0, tiled=True),
    )
    full_in = jnp.dot(wide_in, pieces[0], precision=highest)
    full_out = jnp.dot(wide_out, pieces[1], precision=highest)
    square_in, square_out = lax.psum(
        (jnp.sum(full_in * full_in), jnp.sum(full_out * full_out)), ("fs", "tp")
    )
    entries = float(full_in.shape[0] * full_in.shape[1] * lax.axis_size("fs") * lax.axis_size("tp"))
    update_in = full_in / jnp.sqrt(square_in / entries + 1e-06)
    update_out = full_out / jnp.sqrt(square_out / entries + 1e-06)
    fresh_in = weight_inproj - 0.02 * update_in
    fresh_out = weight_outproj - 0.02 * update_out
    copy_in, copy_out = (
        lax.all_gather(fresh_in.astype(jnp.bfloat16), "fs", axis=0, tiled=True),
        lax.all_gather(fresh_out.astype(jnp.bfloat16), "fs", axis=0, tiled=True),
    )
    return (
        update_in,
        update_out,
        fresh_in,
        fresh_out,
        copy_in,
        copy_out,
        first_in_new,
        first_out_new,
        second_in_new,
        second_out_new,
    )


def solution(mesh):
    return jax.shard_map(
        on_device,
        mesh=mesh,
        in_specs=(
            P("fs", None),
            P("fs", "tp"),
            P("fs", "tp"),
            P("fs", None),
            P("fs", None),
            P("fs", "tp"),
            P("fs", "tp"),
            P("fs", "tp"),
            P("fs", "tp"),
            P("fs", "tp"),
            P("fs", "tp"),
        ),
        out_specs=(
            P("fs", "tp"),
            P("fs", "tp"),
            P("fs", "tp"),
            P("fs", "tp"),
            P(None, "tp"),
            P(None, "tp"),
            P("fs", "tp"),
            P("fs", "tp"),
            P("fs", "tp"),
            P("fs", "tp"),
        ),
        check_vma=False,
    )
```

profile of v0, /device:TPU:0, one launch (start us, length us, event | category | flops | bytes accessed | tf_op | source)
XLA Modules:
  0.0 389.0 jit_solution(17355608462318028329)
XLA Ops:
  9.8 43.4 %all-gather.5.cloned.1.call-done = bf16[2048,256]{1,0:T(8,128)(2,1)} async-done(((bf16[256,256]{1,0:T(8,128)(2,1)}), bf16[2048,256]{1,0:T(8,128)(2,1)}) %all-gather.5.cloned.1.call-update) | async-done | bytes 1048592 | tf_op jit(solution)/shard_map/all_gather | solution.py:32
  53.2 2.3 fusion.6
  55.4 1.5 fusion.7
  57.0 37.3 %all-gather.7.cloned.1.call-done = bf16[2048,256]{1,0:T(8,128)(2,1)} async-done(((bf16[256,256]{1,0:T(8,128)(2,1)}), bf16[2048,256]{1,0:T(8,128)(2,1)}) %all-gather.7.cloned.1.call-update) | async-done | bytes 1048592 | tf_op jit(solution)/shard_map/all_gather | solution.py:33
  94.3 2.3 fusion.8
  96.6 1.5 fusion.9
  98.2 60.9 %reduce-scatter.3.cloned.1.call-done = f32[32,256]{1,0:T(8,128)} async-done(((f32[256,256]{1,0:T(8,128)}), f32[32,256]{1,0:T(8,128)}) %reduce-scatter.3.cloned.1.call-update) | async-done | bytes 32784 | tf_op jit(solution)/shard_map/reduce_scatter | solution.py:40
  159.0 1.4 add_divide_fusion.1
  160.5 30.9 %all_gather.19 = f32[256,256]{1,0:T(8,128)S(1)} all-gather(f32[32,256]{1,0:T(8,128)S(1)} %get-tuple-element.31), channel_id=1, replica_groups=mesh['fs'=8,'tp'=4] {'fs'}, dimensions={0}, use_global_device_ids=true | all-gather | bytes 294912 | tf_op jit(solution)/shard_map/all_gather | solution.py:52
  191.4 1.7 multiply_reduce_fusion.1
  193.1 30.8 %reduce-scatter.5.cloned.1.call-done = f32[32,256]{1,0:T(8,128)} async-done(((f32[256,256]{1,0:T(8,128)}), f32[32,256]{1,0:T(8,128)}) %reduce-scatter.5.cloned.1.call-update) | async-done | bytes 32784 | tf_op jit(solution)/shard_map/reduce_scatter | solution.py:41
  225.3 30.9 %all_gather.21 = f32[256,256]{1,0:T(8,128)S(1)} all-gather(f32[32,256]{1,0:T(8,128)S(1)} %get-tuple-element.28), channel_id=1, replica_groups=mesh['fs'=8,'tp'=4] {'fs'}, dimensions={0}, use_global_device_ids=true | all-gather | bytes 294912 | tf_op jit(solution)/shard_map/all_gather | solution.py:53
  256.2 2.6 multiply_reduce_fusion
  258.8 37.9 %all-reduce = (f32[]{:T(128)}, f32[]{:T(128)}) all-reduce(f32[]{:T(128)} %get-tuple-element.34, f32[]{:T(128)} %get-tuple-element.36), channel_id=1, replica_groups=mesh['fs'=8,'tp'=4] {'fs','tp'}, use_global_device_ids=true, to_apply=%region_2.0 | all-reduce | flops 2 | bytes 16 | tf_op jit(solution)/shard_map/psum | solution.py:57
  297.4 1.8 fusion.3
  299.3 1.8 copy.22
  301.8 1.8 fusion.2
  303.7 1.8 copy.25
  305.4 1.8 copy.23
  307.2 1.8 copy.26
  309.9 29.7 %all-gather.9.cloned.1.call-done = bf16[2048,256]{0,1:T(8,128)(2,1)} async-done(((bf16[256,256]{0,1:T(8,128)(2,1)}), bf16[2048,256]{0,1:T(8,128)(2,1)}) %all-gather.9.cloned.1.call-update) | async-done | bytes 1048592 | tf_op jit(solution)/shard_map/all_gather | solution.py:66
  339.6 2.3 copy.27
  341.8 38.1 %all-gather.11.cloned.1.call-done = bf16[2048,256]{0,1:T(8,128)(2,1)} async-done(((bf16[256,256]{0,1:T(8,128)(2,1)}), bf16[2048,256]{0,1:T(8,128)(2,1)}) %all-gather.11.cloned.1.call-update) | async-done | bytes 1048592 | tf_op jit(solution)/shard_map/all_gather | solution.py:67
  379.9 2.3 copy.28
  (23 shorter events, 5.0 us)
Async XLA Ops:
  7.2 46.0 %copy-start = (bf16[768,2048]{1,0:T(8,128)(2,1)S(1)}, bf16[768,2048]{1,0:T(8,128)(2,1)}, u32[]{:S(2)}) copy-start(bf16[768,2048]{1,0:T(8,128)(2,1)} %param.11) | copy-start | bytes 9437188
  7.2 46.0 %all-gather.5.cloned.1.call-start = ((), (), s32[]{:S(2)}) async-start(), calls=%async_computation.2 | async-start | bytes 1179648 | tf_op jit(solution)/shard_map/all_gather | solution.py:32
  7.9 86.4 %all-gather.7.cloned.1.call-start = ((), (), s32[]{:S(2)}) async-start(), calls=%async_computation.4 | async-start | bytes 1179648 | tf_op jit(solution)/shard_map/all_gather | solution.py:33
  8.7 150.4 %reduce-scatter.3.cloned.1.call-start = ((), (), s32[]{:S(2)}) async-start(), calls=%async_computation.3 | async-start | bytes 294912 | tf_op jit(solution)/shard_map/reduce_scatter | solution.py:40
  53.2 2.3 copy-start.2
  57.0 134.4 %copy-start.1 = (bf16[256,256]{1,0:T(8,128)(2,1)S(1)}, bf16[256,256]{1,0:T(8,128)(2,1)}, u32[]{:S(2)}) copy-start(bf16[256,256]{1,0:T(8,128)(2,1)} %param.14) | copy-start | bytes 393220
  57.0 166.9 %reduce-scatter.5.cloned.1.call-start = ((), (), s32[]{:S(2)}) async-start(), calls=%async_computation.5 | async-start | bytes 294912 | tf_op jit(solution)/shard_map/reduce_scatter | solution.py:41
  94.3 2.3 copy-start.3
  98.1 241.5 %all-gather.9.cloned.1.call-start = ((), (), s32[]{:S(2)}) async-start(), calls=%async_computation.6 | async-start | bytes 1179648 | tf_op jit(solution)/shard_map/all_gather | solution.py:66
  299.3 80.6 %all-gather.11.cloned.1.call-start = ((), (), s32[]{:S(2)}) async-start(), calls=%async_computation.7 | async-start | bytes 1179648 | tf_op jit(solution)/shard_map/all_gather | solution.py:67
Sparse Core Ops, SparseCore 0:
  10.1 42.9 all-gather.4
  55.3 38.9 all-gather.6
  98.2 60.7 reduce-scatter.2
  162.8 61.0 reduce-scatter.4
  299.4 40.1 all-gather.8
  341.5 38.3 all-gather.10
where the time goes:
time: 390 us; the launch traced here: 389 us
  waiting for transfers between devices  242 us (62%)
  blocking collectives  99.7 us (26%)
  between operations  15.6 us (4%)
  local copies, waits for them, and re-layouts  13.6 us (3%)
  matrix products  11.8 us (3%)
  other arithmetic  6.5 us (2%)
    reduce_scatter x1, waiting for transfers between devices, on_device(): lax.psum_scatter(term_in, 'fs', scatter_dimension=0, tiled=True)  60.9 us
    all_gather x1, waiting for transfers between devices, on_device(): lax.all_gather(factor_inproj, 'fs', axis=0, tiled=True)  43.4 us
    all_gather x1, waiting for transfers between devices, on_device(): lax.all_gather(fresh_out.astype(jnp.bfloat16), 'fs', axis=0, tiled=True)  38.1 us
    psum x1, blocking collectives, on_device(): lax.psum((jnp.sum(full_in * full_in), jnp.sum(full_out * full_out)), ('fs...  37.9 us
    all_gather x1, waiting for transfers between devices, on_device(): lax.all_gather(factor_outproj, 'fs', axis=0, tiled=True)  37.3 us
    all_gather x1, blocking collectives, on_device(): lax.all_gather(small_in, 'fs', axis=0, tiled=True)  30.9 us
    all_gather x1, blocking collectives, on_device(): lax.all_gather(small_out, 'fs', axis=0, tiled=True)  30.9 us
    reduce_scatter x1, waiting for transfers between devices, on_device(): lax.psum_scatter(term_out, 'fs', scatter_dimension=0, tiled=True)  30.8 us
  transfers between devices with their start and end apart: 6, of which 6 were waited for; matrix products, arithmetic and copies ran while one was open for 6% of the time, Pallas kernels for 0%

commit v1 on v0

--- a/solution.py
+++ b/solution.py
@@ -1,6 +1,10 @@
+import functools
+
 import jax
 import jax.numpy as jnp
 from jax import lax
+from jax.experimental import pallas as pl
+from jax.experimental.pallas import tpu as pltpu
 from jax.sharding import PartitionSpec as P
 
 
@@ -14,7 +18,7 @@
     )
 
 
-def on_device(
+def plain_form(
     saved_input,
     cot_inproj,
     cot_outproj,
@@ -80,6 +84,361 @@
     )
 
 
+MESH = pl.DeviceIdType.MESH
+F32, BF16 = jnp.float32, jnp.bfloat16
+
+
+def parts_of(x):
+    high = x.astype(BF16)
+    rest = x - high.astype(F32)
+    middle = rest.astype(BF16)
+    return high, middle, (rest - middle.astype(F32)).astype(BF16)
+
+
+def dot(a, b):
+    return jnp.dot(a, b, preferred_element_type=F32)
+
+
+class Gather:
+    def __init__(self, place, chunks, ref_of, sems):
+        self.z, self.y, self.tp, self.depth = place
+        self.chunks, self.ref_of = chunks, ref_of
+        self.up_s, self.up_r, self.dn_s, self.dn_r, self.y_s, self.y_r = sems
+
+    def copy(self, zi, yi, c, s_sem, r_sem, to_z, to_y):
+        ref = self.ref_of(zi * 2 + yi, c)
+        return pltpu.make_async_remote_copy(
+            src_ref=ref, dst_ref=ref, send_sem=s_sem, recv_sem=r_sem,
+            device_id=(to_z * 2 + to_y, self.tp), device_id_type=MESH,
+        )
+
+    def up(self, s, c):
+        return self.copy(self.z - s, self.y, c, self.up_s.at[s, c], self.up_r.at[s, c], self.z + 1, self.y)
+
+    def down(self, s, c):
+        return self.copy(self.z + s, self.y, c, self.dn_s.at[s, c], self.dn_r.at[s, c], self.z - 1, self.y)
+
+    def from_below(self, s, c):
+        return self.copy(self.z - 1 - s, self.y, c, self.up_s.at[s, c], self.up_r.at[s, c], self.z, self.y)
+
+    def from_above(self, s, c):
+        return self.copy(self.z + 1 + s, self.y, c, self.dn_s.at[s, c], self.dn_r.at[s, c], self.z, self.y)
+
+    def across(self, zi, c):
+        return self.copy(zi, self.y, c, self.y_s.at[zi, c], self.y_r.at[zi, c], self.z, 1 - self.y)
+
+    def from_across(self, zi, c):
+        return self.copy(zi, 1 - self.y, c, self.y_s.at[zi, c], self.y_r.at[zi, c], self.z, self.y)
+
+    def start(self, c):
+        @pl.when(self.z + 1 < self.depth)
+        def _():
+            self.up(0, c).start()
+
+        @pl.when(self.z >= 1)
+        def _():
+            self.down(0, c).start()
+
+        self.across(self.z, c).start()
+
+    def relay(self, have=None):
+        have = have or (lambda block, c: None)
+        for s in range(1, self.depth + 1):
+            for c in range(self.chunks):
+                if s < self.depth:
+                    @pl.when(self.z - s >= 0)
+                    def _():
+                        self.from_below(s - 1, c).wait_recv()
+                        if s < self.depth - 1:
+                            @pl.when(self.z + 1 < self.depth)
+                            def _():
+                                self.up(s, c).start()
+                        self.across(self.z - s, c).start()
+                        have((self.z - s) * 2 + self.y, c)
+
+                    @pl.when(self.z + s < self.depth)
+                    def _():
+                        self.from_above(s - 1, c).wait_recv()
+                        if s < self.depth - 1:
+                            @pl.when(self.z >= 1)
+                            def _():
+                                self.down(s, c).start()
+                        self.across(self.z + s, c).start()
+                        have((self.z + s) * 2 + self.y, c)
+
+                if s == 1:
+                    self.from_across(self.z, c).wait_recv()
+                    have(self.z * 2 + 1 - self.y, c)
+                else:
+                    @pl.when(self.z - (s - 1) >= 0)
+                    def _():
+                        self.from_across(self.z - (s - 1), c).wait_recv()
+                        have((self.z - (s - 1)) * 2 + 1 - self.y, c)
+
+                    @pl.when(self.z + (s - 1) < self.depth)
+                    def _():
+                        self.from_across(self.z + (s - 1), c).wait_recv()
+                        have((self.z + (s - 1)) * 2 + 1 - self.y, c)
+
+    def finish(self):
+        for c in range(self.chunks):
+            for s in range(self.depth - 1):
+                @pl.when((self.z - s >= 0) & (self.z + 1 < self.depth))
+                def _():
+                    self.up(s, c).wait_send()
+
+                @pl.when((self.z + s < self.depth) & (self.z >= 1))
+                def _():
+                    self.down(s, c).wait_send()
+            for zi in range(self.depth):
+                self.across(zi, c).wait_send()
+
+
+def gather_sems(depth, chunks):
+    dma = pltpu.SemaphoreType.DMA
+    return [dma((depth - 1, chunks))] * 4 + [dma((depth, chunks))] * 2
+
+
+def kernel(
+    n, tps, entries,
+    saved_hbm, cot_in_hbm, cot_out_hbm, factor_in_hbm, factor_out_hbm, weight_in_hbm, weight_out_hbm,
+    first_in_hbm, first_out_hbm, second_in_hbm, second_out_hbm,
+    update, fresh, copies, first_new, second_new,
+    saved, cots, factors, weights, first, second, mapped, terms, landed, smalls, squares,
+    load_sem, f_upS, f_upR, f_dnS, f_dnR, f_yS, f_yR, pair_s, pair_r, term_s, term_r,
+    s_upS, s_upR, s_dnS, s_dnR, s_yS, s_yR, norm_s, norm_r,
+    c_upS, c_upR, c_dnS, c_dnR, c_yS, c_yR,
+):
+    me, tp = lax.axis_index("fs"), lax.axis_index("tp")
+    z, y = me // 2, me % 2
+    depth = n // 2
+    side = tp % 2
+    partner = tp + 1 - 2 * side
+    rows = factors.shape[2]
+    slim = first.shape[1]
+    place = (z, y, tp, depth)
+
+    barrier = pltpu.get_barrier_semaphore()
+    for k in range(1, n):
+        pl.semaphore_signal(barrier, inc=1, device_id=((me + k) % n, tp), device_id_type=MESH)
+    for k in range(1, tps):
+        pl.semaphore_signal(barrier, inc=1, device_id=(me, (tp + k) % tps), device_id_type=MESH)
+
+    loads = [
+        pltpu.make_async_copy(source, target, load_sem.at[i])
+        for i, (source, target) in enumerate((
+            (factor_in_hbm, factors.at[0, me]), (factor_out_hbm, factors.at[1, me]),
+            (saved_hbm, saved), (cot_in_hbm, cots.at[0]), (cot_out_hbm, cots.at[1]),
+            (first_in_hbm, first.at[0]), (first_out_hbm, first.at[1]),
+            (second_in_hbm, second.at[0]), (second_out_hbm, second.at[1]),
+            (weight_in_hbm, weights.at[0]), (weight_out_hbm, weights.at[1]),
+        ))
+    ]
+    for load in loads:
+        load.start()
+    loads[0].wait()
+    loads[1].wait()
+    pl.semaphore_wait(barrier, n - 1 + tps - 1)
+
+    def hand(block):
+        ref = factors.at[side, block]
+        return pltpu.make_async_remote_copy(
+            src_ref=ref, dst_ref=ref, send_sem=pair_s.at[block], recv_sem=pair_r.at[block],
+            device_id=(me, partner), device_id_type=MESH,
+        )
+
+    def handed(block):
+        ref = factors.at[1 - side, block]
+        return pltpu.make_async_remote_copy(
+            src_ref=ref, dst_ref=ref, send_sem=pair_s.at[block], recv_sem=pair_r.at[block],
+            device_id=(me, tp), device_id_type=MESH,
+        )
+
+    gather = Gather(place, 1, lambda block, c: factors.at[side, block], (f_upS, f_upR, f_dnS, f_dnR, f_yS, f_yR))
+    gather.start(0)
+    loads[2].wait()
+
+    def map_block(block, first_one):
+        piece = saved[:, pl.ds(pl.multiple_of(block * rows, rows), rows)]
+        for m in range(2):
+            product = dot(piece, factors[m, block])
+            mapped[m] = product if first_one else mapped[m] + product
+
+    map_block(me, True)
+    gather.relay(lambda block, c: hand(block).start())
+    for k in range(1, n):
+        block = (me + k) % n
+        handed(block).wait_recv()
+        map_block(block, False)
+
+    for load in loads[3:]:
+        load.wait()
+    for m in range(2):
+        high, middle, low = parts_of(mapped[m].T)
+        term = dot(high, cots[m]) + (dot(middle, cots[m]) + dot(low, cots[m]))
+        terms[:, m * slim:(m + 1) * slim, :] = term.reshape(n, slim, term.shape[1])
+
+    def send_term(k):
+        return pltpu.make_async_remote_copy(
+            src_ref=terms.at[(me + k) % n], dst_ref=landed.at[me], send_sem=term_s.at[k], recv_sem=term_r.at[k],
+            device_id=((me + k) % n, tp), device_id_type=MESH,
+        )
+
+    def recv_term(k):
+        return pltpu.make_async_remote_copy(
+            src_ref=terms.at[me], dst_ref=landed.at[(me + n - k) % n], send_sem=term_s.at[k], recv_sem=term_r.at[k],
+            device_id=(me, tp), device_id_type=MESH,
+        )
+
+    for k in range(1, n):
+        send_term(k).start()
+    projected = terms[me]
+    for k in range(1, n):
+        recv_term(k).wait_recv()
+        projected = projected + landed[(me + n - k) % n]
+    for m in range(2):
+        here = projected[m * slim:(m + 1) * slim]
+        first_m = 0.8 * first[m] + 0.2 * here
+        second_m = 0.9 * second[m] + 0.1 * here * here
+        first_new[m] = first_m
+        second_new[m] = second_m
+        smalls[me, m * slim:(m + 1) * slim, :] = first_m / (jnp.sqrt(second_m) + 1e-08)
+
+    small_gather = Gather(place, 1, lambda block, c: smalls.at[block], (s_upS, s_upR, s_dnS, s_dnR, s_yS, s_yR))
+    small_gather.start(0)
+    small_gather.relay()
+
+    small_parts = [
+        parts_of(smalls[:, m * slim:(m + 1) * slim, :].reshape(n * slim, smalls.shape[2])) for m in range(2)
+    ]
+
+    def full_of(m, block):
+        high, middle, low = small_parts[m]
+        factor = factors[m, block]
+        return dot(factor, high) + (dot(factor, middle) + dot(factor, low))
+
+    for m in range(2):
+        total = None
+        for block in range(n):
+            full = full_of(m, block)
+            square = jnp.sum((full * full).reshape(rows // 8, 8, full.shape[1]), axis=0)
+            total = square if total is None else total + square
+        squares[tp, m] = total
+
+    def send_square(k):
+        return pltpu.make_async_remote_copy(
+            src_ref=squares.at[tp], dst_ref=squares.at[tp], send_sem=norm_s.at[k], recv_sem=norm_r.at[k],
+            device_id=(me, (tp + k) % tps), device_id_type=MESH,
+        )
+
+    def recv_square(k):
+        ref = squares.at[(tp + tps - k) % tps]
+        return pltpu.make_async_remote_copy(
+            src_ref=ref, dst_ref=ref, send_sem=norm_s.at[k], recv_sem=norm_r.at[k],
+            device_id=(me, tp), device_id_type=MESH,
+        )
+
+    for k in range(1, tps):
+        send_square(k).start()
+    for m in range(2):
+        update[m] = full_of(m, me)
+    for k in range(1, tps):
+        recv_square(k).wait_recv()
+    copy_gather = Gather(place, 2, lambda block, c: copies.at[c, block], (c_upS, c_upR, c_dnS, c_dnR, c_yS, c_yR))
+    for m in range(2):
+        mean = jnp.sum(jnp.sum(squares[:, m], axis=0), keepdims=True) / entries
+        new_update = update[m] / jnp.sqrt(mean + 1e-06)
+        update[m] = new_update
+        new_weight = weights[m] - 0.02 * new_update
+        fresh[m] = new_weight
+        copies[m, me] = new_weight.astype(BF16)
+        copy_gather.start(m)
+    copy_gather.relay()
+
+    gather.finish()
+    small_gather.finish()
+    copy_gather.finish()
+    for k in range(1, n):
+        hand((me + k) % n).wait_send()
+        send_term(k).wait_send()
+    for k in range(1, tps):
+        send_square(k).wait_send()
+
+
+def write_kernel(update, fresh, copies, first_new, second_new, *refs):
+    outs, sem = refs[:-1], refs[-1]
+    count = 0
+    started = []
+    for i, source in enumerate((update, fresh, copies, first_new, second_new)):
+        for m in range(2):
+            copy = pltpu.make_async_copy(source.at[m], outs[2 * i + m], sem.at[count])
+            copy.start()
+            started.append(copy)
+            count += 1
+    for copy in started:
+        copy.wait()
+
+
+def kernel_form(n, tps, saved_input, cot_inproj, cot_outproj, factor_inproj, *others):
+    tokens, wide = saved_input.shape
+    columns = cot_inproj.shape[1]
+    rows, rank = factor_inproj.shape
+    slim = rank // n
+    depth = n // 2
+    entries = float(wide * columns * tps)
+    dma = pltpu.SemaphoreType.DMA
+    vmem = pl.BlockSpec(memory_space=pltpu.VMEM)
+    anywhere = pl.BlockSpec(memory_space=pl.ANY)
+    shape = jax.ShapeDtypeStruct
+    results = pl.pallas_call(
+        functools.partial(kernel, n, tps, entries),
+        out_shape=(
+            shape((2, rows, columns), F32), shape((2, rows, columns), F32),
+            shape((2, n, rows, columns), BF16),
+            shape((2, slim, columns), F32), shape((2, slim, columns), F32),
+        ),
+        in_specs=[anywhere] * 11,
+        out_specs=[vmem] * 5,
+        scratch_shapes=[
+            pltpu.VMEM((tokens, wide), BF16),
+            pltpu.VMEM((2, tokens, columns), BF16),
+            pltpu.VMEM((2, n, rows, rank), BF16),
+            pltpu.VMEM((2, rows, columns), F32),
+            pltpu.VMEM((2, slim, columns), F32),
+            pltpu.VMEM((2, slim, columns), F32),
+            pltpu.VMEM((2, tokens, rank), F32),
+            pltpu.VMEM((n, 2 * slim, columns), F32),
+            pltpu.VMEM((n, 2 * slim, columns), F32),
+            pltpu.VMEM((n, 2 * slim, columns), F32),
+            pltpu.VMEM((tps, 2, 8, columns), F32),
+            dma((11,)),
+            *gather_sems(depth, 1), dma((n,)), dma((n,)), dma((n,)), dma((n,)),
+            *gather_sems(depth, 1), dma((tps,)), dma((tps,)),
+            *gather_sems(depth, 2),
+        ],
+        compiler_params=pltpu.CompilerParams(collective_id=0, has_side_effects=True, vmem_limit_bytes=48 * 2**20),
+    )(saved_input, cot_inproj, cot_outproj, factor_inproj, *others)
+    update, fresh, copies, first_new, second_new = results
+    copies = copies.reshape(2, n * rows, columns)
+    return pl.pallas_call(
+        write_kernel,
+        out_shape=(
+            *[shape((rows, columns), F32)] * 4, *[shape((n * rows, columns), BF16)] * 2, *[shape((slim, columns), F32)] * 4,
+        ),
+        in_specs=[vmem] * 5,
+        out_specs=[anywhere] * 10,
+        scratch_shapes=[dma((10,))],
+    )(update, fresh, copies, first_new, second_new)
+
+
+def on_device(saved_input, cot_inproj, cot_outproj, factor_inproj, *others):
+    n, tps = lax.axis_size("fs"), lax.axis_size("tp")
+    rows, rank = factor_inproj.shape
+    if n % 2 == 0 and n >= 4 and tps % 2 == 0 and rank % (8 * n) == 0 and rows % 128 == 0 and cot_inproj.shape[1] % 128 == 0:
+        return kernel_form(n, tps, saved_input, cot_inproj, cot_outproj, factor_inproj, *others)
+    return plain_form(saved_input, cot_inproj, cot_outproj, factor_inproj, *others)
+
+
 def solution(mesh):
     return jax.shard_map(
         on_device,

time: 390 us -> 97.8 us (0.25)
  waiting for transfers between devices: 242 us -> 0 us
  blocking collectives: 99.7 us -> 0 us
  Pallas kernels: 0 us -> 83.6 us
  between operations: 15.6 us -> 0.69 us
  matrix products: 11.8 us -> 0 us
  other arithmetic: 6.5 us -> 0 us
    all_gather x4 -> x0, waiting for transfers between devices: 148 us -> none  [the longest x1 43.4 us: on_device(): lax.all_gather(factor_inproj, 'fs', axis=0, tiled=True)]
    reduce_scatter x2 -> x0, waiting for transfers between devices: 91.7 us -> none  [the longest x1 60.9 us: on_device(): lax.psum_scatter(term_in, 'fs', scatter_dimension=0, tiled=True)]
    pallas_call x0 -> x2, Pallas kernels: none -> 83.6 us  [the longest x1 79.9 us: kernel_form(): pl.pallas_call(functools.partial(kernel, n, tps, entries), out_shape=(sha...]
    all_gather x2 -> x0, blocking collectives: 61.8 us -> none  [the longest x1 30.9 us: on_device(): lax.all_gather(small_in, 'fs', axis=0, tiled=True)]
    psum x1 -> x0, blocking collectives: 37.9 us -> none  [on_device(): lax.psum((jnp.sum(full_in * full_in), jnp.sum(full_out * full_out)), ('fs...]
    dot_general x6 -> x0, matrix products: 11.8 us -> none  [the longest x2 3 us: contract_rows(): lax.dot_general(left, right, (((0,), (0,)), ((), ())), precision=precisio...]
    unnamed x16 -> x30, local copies, waits for them, and re-layouts: 13.6 us -> 12.9 us
  transfers between devices with their start and end apart: 6 -> 0, of which waited for: 6 -> 0; matrix products, arithmetic and copies ran while one was open for 6% -> 0% of each run, Pallas kernels for 0% -> 0%
where the time goes in v1:
time: 97.8 us; the launch traced here: 97.2 us
  Pallas kernels  83.6 us (85%)
  local copies, waits for them, and re-layouts  12.9 us (13%)
    pallas_call x1, Pallas kernels, kernel_form(): pl.pallas_call(functools.partial(kernel, n, tps, entries), out_shape=(sha...  79.9 us
    unnamed x30, local copies, waits for them, and re-layouts  12.9 us
    pallas_call x1, Pallas kernels, kernel_form(): pl.pallas_call(write_kernel, out_shape=(*[shape((rows, columns), F32)] *...  3.71 us

profile of v1, /device:TPU:0, one launch (start us, length us, event | category | flops | bytes accessed | tf_op | source)
XLA Modules:
  0.0 97.2 jit_solution(15825171302359046637)
XLA Ops:
  0.6 0.0 copy-start.3
  0.7 1.0 %copy-done.3 = bf16[768,256]{1,0:T(8,128)(2,1)S(1)} copy-done((bf16[768,256]{1,0:T(8,128)(2,1)S(1)}, bf16[768,256]{1,0:T(8,128)(2,1)}, u32[]{:S(2)}) %copy-start.3) | copy-done | bytes 393240
  1.6 0.0 copy-start.4
  1.6 1.0 %copy-done.4 = bf16[768,256]{1,0:T(8,128)(2,1)S(1)} copy-done((bf16[768,256]{1,0:T(8,128)(2,1)S(1)}, bf16[768,256]{1,0:T(8,128)(2,1)}, u32[]{:S(2)}) %copy-start.4) | copy-done | bytes 393240
  2.6 0.0 copy-start.5
  2.6 0.9 copy-done.5
  3.6 0.0 copy-start.6
  3.6 0.9 copy-done.6
  4.5 0.0 copy-start.7
  4.5 0.9 copy-done.7
  5.4 0.0 copy-start.8
  5.4 0.9 copy-done.8
  6.4 0.8 copy-done.11
  7.1 0.8 copy-done.12
  7.9 0.8 copy-done.13
  8.6 0.8 copy-done.14
  9.4 79.9 %shard_map.186 = (f32[2,256,256]{2,1,0:T(8,128)S(1)}, f32[2,256,256]{2,1,0:T(8,128)S(1)}, bf16[2,8,256,256]{3,2,1,0:T(8,128)(2,1)S(1)}, f32[2,32,256]{2,1,0:T(8,128)S(1)}, f32[2,32,256]{2,1,0:T(8,128)S(1)}) custom-call(bf16[768,2048]{1,0:T(8,128)(2,1)} %saved_hbm.1, bf16[768,256]{1,0:T(8,128)(2,1)S(1)} %copy-done.3, bf16[768,256]{1,0:T(8,128)(2,1)S(1)} %copy-done.4, ...), custom_call_target="tpu_custom_call" | custom-call | tf_op jit(solution)/shard_map/pallas_call | solution.py:393
  89.3 0.0 copy-start
  89.3 1.3 %copy-done = bf16[2,8,256,256]{3,2,1,0:T(8,128)(2,1)} copy-done((bf16[2,8,256,256]{3,2,1,0:T(8,128)(2,1)}, bf16[2,8,256,256]{3,2,1,0:T(8,128)(2,1)S(1)}, u32[]{:S(2)}) %copy-start) | copy-done | bytes 2097176
  90.6 0.8 copy-done.1
  91.4 0.8 copy-done.2
  92.2 0.6 copy-done.9
  92.9 0.6 copy-done.10
  93.5 3.7 %shard_map.187 = (f32[256,256]{1,0:T(8,128)}, f32[256,256]{1,0:T(8,128)}, f32[256,256]{1,0:T(8,128)}, f32[256,256]{1,0:T(8,128)}, bf16[2048,256]{1,0:T(8,128)(2,...) custom-call(f32[2,256,256]{2,1,0:T(8,128)} %copy-done.1, ...), custom_call_target="tpu_custom_call" | custom-call | tf_op jit(solution)/shard_map/pallas_call | solution.py:423
  (8 shorter events, 0.0 us)
Async XLA Ops:
  0.6 1.0 %copy-start.3 = (bf16[768,256]{1,0:T(8,128)(2,1)S(1)}, bf16[768,256]{1,0:T(8,128)(2,1)}, u32[]{:S(2)}) copy-start(bf16[768,256]{1,0:T(8,128)(2,1)} %cot_in_hbm.1) | copy-start | bytes 1179652
  1.6 1.0 %copy-start.4 = (bf16[768,256]{1,0:T(8,128)(2,1)S(1)}, bf16[768,256]{1,0:T(8,128)(2,1)}, u32[]{:S(2)}) copy-start(bf16[768,256]{1,0:T(8,128)(2,1)} %cot_out_hbm.1) | copy-start | bytes 1179652
  2.6 0.9 copy-start.5
  3.6 0.9 copy-start.6
  4.5 0.9 copy-start.7
  5.4 0.9 copy-start.8
  6.4 0.8 copy-start.11
  7.1 0.8 copy-start.12
  7.9 0.8 copy-start.13
  8.6 0.8 copy-start.14
  89.3 1.3 %copy-start = (bf16[2,8,256,256]{3,2,1,0:T(8,128)(2,1)}, bf16[2,8,256,256]{3,2,1,0:T(8,128)(2,1)S(1)}, u32[]{:S(2)}) copy-start(bf16[2,8,256,256]{3,2,1,0:T(8,128)(2,1)S(1)} %get-tuple-element.17) | copy-start | bytes 6291460
  90.6 0.8 copy-start.1
  91.4 0.8 copy-start.2
  92.2 0.6 copy-start.9
  92.8 0.6 copy-start.10

commit v2 on v1

--- a/solution.py
+++ b/solution.py
@@ -103,7 +103,16 @@
     def __init__(self, place, chunks, ref_of, sems):
         self.z, self.y, self.tp, self.depth = place
         self.chunks, self.ref_of = chunks, ref_of
-        self.up_s, self.up_r, self.dn_s, self.dn_r, self.y_s, self.y_r = sems
+        self.up_s, self.up_r, self.dn_s, self.dn_r, self.y_s, self.y_r, self.x_s, self.x_r = sems
+
+    def detour(self, zi, c):
+        z, last = self.z, self.depth - 1
+        if self.depth < 4:
+            return z < 0
+        end = ((z == 1) & (zi == 0)) | ((z == last - 1) & (zi == last))
+        if c == self.chunks - 1:
+            end = end | ((z == 0) & (zi == 1)) | ((z == last) & (zi == last - 1))
+        return end
 
     def copy(self, zi, yi, c, s_sem, r_sem, to_z, to_y):
         ref = self.ref_of(zi * 2 + yi, c)
@@ -130,6 +139,21 @@
     def from_across(self, zi, c):
         return self.copy(zi, 1 - self.y, c, self.y_s.at[zi, c], self.y_r.at[zi, c], self.z, self.y)
 
+    def beside(self, c, to_z):
+        return self.copy(self.z, 1 - self.y, c, self.x_s.at[c], self.x_r.at[c], to_z, self.y)
+
+    def from_beside(self, zi, c):
+        return self.copy(zi, 1 - self.y, c, self.x_s.at[c], self.x_r.at[c], self.z, self.y)
+
+    def beside_cases(self, c):
+        if self.depth < 4:
+            return ()
+        z, last = self.z, self.depth - 1
+        cases = [(z == 0, 1), (z == last, last - 1)]
+        if c == self.chunks - 1:
+            cases += [(z == 1, 0), (z == last - 1, last)]
+        return cases
+
     def start(self, c):
         @pl.when(self.z + 1 < self.depth)
         def _():
@@ -141,44 +165,67 @@
 
         self.across(self.z, c).start()
 
-    def relay(self, have=None):
+    def hand_on(self, zi, c):
+        @pl.when(jnp.logical_not(self.detour(zi, c)))
+        def _():
+            self.across(zi, c).start()
+
+    def land(self, zi, c, have):
+        gone = self.detour(zi, c)
+
+        @pl.when(gone)
+        def _():
+            self.from_beside(zi, c).wait_recv()
+
+        @pl.when(jnp.logical_not(gone))
+        def _():
+            self.from_across(zi, c).wait_recv()
+
+        have(zi * 2 + 1 - self.y, c)
+
+    def relay(self, have=None, after=None):
         have = have or (lambda block, c: None)
-        for s in range(1, self.depth + 1):
+        z, depth = self.z, self.depth
+        for s in range(1, depth + 1):
             for c in range(self.chunks):
-                if s < self.depth:
-                    @pl.when(self.z - s >= 0)
+                if s < depth:
+                    @pl.when(z - s >= 0)
                     def _():
                         self.from_below(s - 1, c).wait_recv()
-                        if s < self.depth - 1:
-                            @pl.when(self.z + 1 < self.depth)
+                        if s < depth - 1:
+                            @pl.when(z + 1 < depth)
                             def _():
                                 self.up(s, c).start()
-                        self.across(self.z - s, c).start()
-                        have((self.z - s) * 2 + self.y, c)
-
-                    @pl.when(self.z + s < self.depth)
+                        self.hand_on(z - s, c)
+                        have((z - s) * 2 + self.y, c)
+
+                    @pl.when(z + s < depth)
                     def _():
                         self.from_above(s - 1, c).wait_recv()
-                        if s < self.depth - 1:
-                            @pl.when(self.z >= 1)
+                        if s < depth - 1:
+                            @pl.when(z >= 1)
                             def _():
                                 self.down(s, c).start()
-                        self.across(self.z + s, c).start()
-                        have((self.z + s) * 2 + self.y, c)
+                        self.hand_on(z + s, c)
+                        have((z + s) * 2 + self.y, c)
 
                 if s == 1:
-                    self.from_across(self.z, c).wait_recv()
-                    have(self.z * 2 + 1 - self.y, c)
+                    self.from_across(z, c).wait_recv()
+                    for condition, neighbour in self.beside_cases(c):
+                        @pl.when(condition)
+                        def _():
+                            self.beside(c, neighbour).start()
+                    have(z * 2 + 1 - self.y, c)
                 else:
-                    @pl.when(self.z - (s - 1) >= 0)
+                    @pl.when(z - (s - 1) >= 0)
                     def _():
-                        self.from_across(self.z - (s - 1), c).wait_recv()
-                        have((self.z - (s - 1)) * 2 + 1 - self.y, c)
-
-                    @pl.when(self.z + (s - 1) < self.depth)
+                        self.land(z - (s - 1), c, have)
+
+                    @pl.when(z + (s - 1) < depth)
                     def _():
-                        self.from_across(self.z + (s - 1), c).wait_recv()
-                        have((self.z + (s - 1)) * 2 + 1 - self.y, c)
+                        self.land(z + (s - 1), c, have)
+            if after is not None:
+                after(s)
 
     def finish(self):
         for c in range(self.chunks):
@@ -191,12 +238,18 @@
                 def _():
                     self.down(s, c).wait_send()
             for zi in range(self.depth):
-                self.across(zi, c).wait_send()
+                @pl.when(jnp.logical_not(self.detour(zi, c)))
+                def _():
+                    self.across(zi, c).wait_send()
+            for condition, neighbour in self.beside_cases(c):
+                @pl.when(condition)
+                def _():
+                    self.beside(c, neighbour).wait_send()
 
 
 def gather_sems(depth, chunks):
     dma = pltpu.SemaphoreType.DMA
-    return [dma((depth - 1, chunks))] * 4 + [dma((depth, chunks))] * 2
+    return [dma((depth - 1, chunks))] * 4 + [dma((depth, chunks))] * 2 + [dma((chunks,))] * 2
 
 
 def kernel(
@@ -204,10 +257,8 @@
     saved_hbm, cot_in_hbm, cot_out_hbm, factor_in_hbm, factor_out_hbm, weight_in_hbm, weight_out_hbm,
     first_in_hbm, first_out_hbm, second_in_hbm, second_out_hbm,
     update, fresh, copies, first_new, second_new,
-    saved, cots, factors, weights, first, second, mapped, terms, landed, smalls, squares,
-    load_sem, f_upS, f_upR, f_dnS, f_dnR, f_yS, f_yR, pair_s, pair_r, term_s, term_r,
-    s_upS, s_upR, s_dnS, s_dnR, s_yS, s_yR, norm_s, norm_r,
-    c_upS, c_upR, c_dnS, c_dnR, c_yS, c_yR,
+    saved, cots, factors, weights, first, second, mapped, terms, crossed, staged, landed, smalls, squares,
+    load_sem, pair_s, pair_r, ty_s, ty_r, tz_s, tz_r, sz_s, sz_r, sy_s, sy_r, norm_s, norm_r, *gather_refs,
 ):
     me, tp = lax.axis_index("fs"), lax.axis_index("tp")
     z, y = me // 2, me % 2
@@ -215,12 +266,14 @@
     side = tp % 2
     partner = tp + 1 - 2 * side
     rows = factors.shape[2]
+    half = rows // 2
     slim = first.shape[1]
     place = (z, y, tp, depth)
 
     barrier = pltpu.get_barrier_semaphore()
-    for k in range(1, n):
-        pl.semaphore_signal(barrier, inc=1, device_id=((me + k) % n, tp), device_id_type=MESH)
+    for k in range(1, depth):
+        pl.semaphore_signal(barrier, inc=1, device_id=((z + k) % depth * 2 + y, tp), device_id_type=MESH)
+    pl.semaphore_signal(barrier, inc=1, device_id=(z * 2 + 1 - y, tp), device_id_type=MESH)
     for k in range(1, tps):
         pl.semaphore_signal(barrier, inc=1, device_id=(me, (tp + k) % tps), device_id_type=MESH)
 
@@ -238,115 +291,169 @@
         load.start()
     loads[0].wait()
     loads[1].wait()
-    pl.semaphore_wait(barrier, n - 1 + tps - 1)
-
-    def hand(block):
-        ref = factors.at[side, block]
-        return pltpu.make_async_remote_copy(
-            src_ref=ref, dst_ref=ref, send_sem=pair_s.at[block], recv_sem=pair_r.at[block],
+    pl.semaphore_wait(barrier, depth + tps - 1)
+
+    def factor_ref(m, block, c):
+        return factors.at[m, block, pl.ds(c * half, half)]
+
+    def hand(m, block, c):
+        ref = factor_ref(m, block, c)
+        return pltpu.make_async_remote_copy(
+            src_ref=ref, dst_ref=ref, send_sem=pair_s.at[block, c], recv_sem=pair_r.at[block, c],
             device_id=(me, partner), device_id_type=MESH,
         )
 
-    def handed(block):
-        ref = factors.at[1 - side, block]
-        return pltpu.make_async_remote_copy(
-            src_ref=ref, dst_ref=ref, send_sem=pair_s.at[block], recv_sem=pair_r.at[block],
-            device_id=(me, tp), device_id_type=MESH,
-        )
-
-    gather = Gather(place, 1, lambda block, c: factors.at[side, block], (f_upS, f_upR, f_dnS, f_dnR, f_yS, f_yR))
+    gather = Gather(place, 2, lambda block, c: factor_ref(side, block, c), gather_refs[:8])
     gather.start(0)
+    gather.start(1)
     loads[2].wait()
 
-    def map_block(block, first_one):
+    def map_block(block, first_one=False):
         piece = saved[:, pl.ds(pl.multiple_of(block * rows, rows), rows)]
         for m in range(2):
             product = dot(piece, factors[m, block])
             mapped[m] = product if first_one else mapped[m] + product
 
+    def map_handed(block):
+        for c in range(2):
+            hand(1 - side, block, c).wait_recv()
+        map_block(block)
+
+    def map_at(distance):
+        if distance == 0:
+            map_handed(z * 2 + 1 - y)
+            return
+
+        @pl.when(z - distance >= 0)
+        def _():
+            map_handed((z - distance) * 2 + y)
+            map_handed((z - distance) * 2 + 1 - y)
+
+        @pl.when(z + distance < depth)
+        def _():
+            map_handed((z + distance) * 2 + y)
+            map_handed((z + distance) * 2 + 1 - y)
+
     map_block(me, True)
-    gather.relay(lambda block, c: hand(block).start())
-    for k in range(1, n):
-        block = (me + k) % n
-        handed(block).wait_recv()
-        map_block(block, False)
-
+    gather.relay(
+        lambda block, c: hand(side, block, c).start(),
+        lambda s: map_at(s - 2) if s >= 2 else None,
+    )
+    map_at(depth - 1)
+
+    def term_cross(m, zi):
+        return pltpu.make_async_remote_copy(
+            src_ref=terms.at[m, zi * 2 + 1 - y], dst_ref=crossed.at[m, zi],
+            send_sem=ty_s.at[m, zi], recv_sem=ty_r.at[m, zi],
+            device_id=(z * 2 + 1 - y, tp), device_id_type=MESH,
+        )
+
+    def term_along(m, zi):
+        return pltpu.make_async_remote_copy(
+            src_ref=staged.at[m, zi], dst_ref=landed.at[m, z], send_sem=tz_s.at[m, zi], recv_sem=tz_r.at[m, z],
+            device_id=(zi * 2 + y, tp), device_id_type=MESH,
+        )
+
+    def term_from(m, zi):
+        return pltpu.make_async_remote_copy(
+            src_ref=staged.at[m, z], dst_ref=landed.at[m, zi], send_sem=tz_s.at[m, z], recv_sem=tz_r.at[m, zi],
+            device_id=(z * 2 + y, tp), device_id_type=MESH,
+        )
+
+    order = [k % depth for k in range(1, depth + 1)]
     for load in loads[3:]:
         load.wait()
     for m in range(2):
         high, middle, low = parts_of(mapped[m].T)
         term = dot(high, cots[m]) + (dot(middle, cots[m]) + dot(low, cots[m]))
-        terms[:, m * slim:(m + 1) * slim, :] = term.reshape(n, slim, term.shape[1])
-
-    def send_term(k):
-        return pltpu.make_async_remote_copy(
-            src_ref=terms.at[(me + k) % n], dst_ref=landed.at[me], send_sem=term_s.at[k], recv_sem=term_r.at[k],
-            device_id=((me + k) % n, tp), device_id_type=MESH,
-        )
-
-    def recv_term(k):
-        return pltpu.make_async_remote_copy(
-            src_ref=terms.at[me], dst_ref=landed.at[(me + n - k) % n], send_sem=term_s.at[k], recv_sem=term_r.at[k],
-            device_id=(me, tp), device_id_type=MESH,
-        )
-
-    for k in range(1, n):
-        send_term(k).start()
-    projected = terms[me]
-    for k in range(1, n):
-        recv_term(k).wait_recv()
-        projected = projected + landed[(me + n - k) % n]
-    for m in range(2):
-        here = projected[m * slim:(m + 1) * slim]
+        terms[m] = term.reshape(n, slim, term.shape[1])
+        for k in order:
+            term_cross(m, (z + k) % depth).start()
+    for m in range(2):
+        for k in order:
+            zi = (z + k) % depth
+            term_cross(m, zi).wait_recv()
+            staged[m, zi] = terms[m, zi * 2 + y] + crossed[m, zi]
+            if k:
+                term_along(m, zi).start()
+
+    def small_along(m, zi):
+        ref = smalls.at[m, me]
+        return pltpu.make_async_remote_copy(
+            src_ref=ref, dst_ref=ref, send_sem=sz_s.at[m, zi], recv_sem=sz_r.at[m, z],
+            device_id=(zi * 2 + y, tp), device_id_type=MESH,
+        )
+
+    def small_from(m, zi):
+        ref = smalls.at[m, zi * 2 + y]
+        return pltpu.make_async_remote_copy(
+            src_ref=ref, dst_ref=ref, send_sem=sz_s.at[m, zi], recv_sem=sz_r.at[m, zi],
+            device_id=(z * 2 + y, tp), device_id_type=MESH,
+        )
+
+    def small_cross(m, zi, column):
+        ref = smalls.at[m, zi * 2 + column]
+        return pltpu.make_async_remote_copy(
+            src_ref=ref, dst_ref=ref, send_sem=sy_s.at[m, zi], recv_sem=sy_r.at[m, zi],
+            device_id=(z * 2 + 1 - y, tp), device_id_type=MESH,
+        )
+
+    for m in range(2):
+        here = staged[m, z]
+        for k in range(1, depth):
+            term_from(m, (z + k) % depth).wait_recv()
+            here = here + landed[m, (z + k) % depth]
         first_m = 0.8 * first[m] + 0.2 * here
         second_m = 0.9 * second[m] + 0.1 * here * here
         first_new[m] = first_m
         second_new[m] = second_m
-        smalls[me, m * slim:(m + 1) * slim, :] = first_m / (jnp.sqrt(second_m) + 1e-08)
-
-    small_gather = Gather(place, 1, lambda block, c: smalls.at[block], (s_upS, s_upR, s_dnS, s_dnR, s_yS, s_yR))
-    small_gather.start(0)
-    small_gather.relay()
-
-    small_parts = [
-        parts_of(smalls[:, m * slim:(m + 1) * slim, :].reshape(n * slim, smalls.shape[2])) for m in range(2)
-    ]
-
-    def full_of(m, block):
-        high, middle, low = small_parts[m]
-        factor = factors[m, block]
-        return dot(factor, high) + (dot(factor, middle) + dot(factor, low))
-
-    for m in range(2):
+        smalls[m, me] = first_m / (jnp.sqrt(second_m) + 1e-08)
+        for k in range(1, depth):
+            small_along(m, (z + k) % depth).start()
+        small_cross(m, z, y).start()
+    for m in range(2):
+        for k in range(1, depth):
+            zi = (z + k) % depth
+            small_from(m, zi).wait_recv()
+            small_cross(m, zi, y).start()
+
+    def send_square(m, k):
+        return pltpu.make_async_remote_copy(
+            src_ref=squares.at[m, tp], dst_ref=squares.at[m, tp], send_sem=norm_s.at[m, k], recv_sem=norm_r.at[m, k],
+            device_id=(me, (tp + k) % tps), device_id_type=MESH,
+        )
+
+    def recv_square(m, k):
+        ref = squares.at[m, (tp + tps - k) % tps]
+        return pltpu.make_async_remote_copy(
+            src_ref=ref, dst_ref=ref, send_sem=norm_s.at[m, k], recv_sem=norm_r.at[m, k],
+            device_id=(me, tp), device_id_type=MESH,
+        )
+
+    for m in range(2):
+        for k in range(depth):
+            small_cross(m, (z + k) % depth, 1 - y).wait_recv()
+        high, middle, low = parts_of(smalls[m].reshape(n * slim, smalls.shape[3]))
+
+        def full_of(block):
+            factor = factors[m, block]
+            return dot(factor, high) + (dot(factor, middle) + dot(factor, low))
+
         total = None
         for block in range(n):
-            full = full_of(m, block)
+            full = full_of(block)
             square = jnp.sum((full * full).reshape(rows // 8, 8, full.shape[1]), axis=0)
             total = square if total is None else total + square
-        squares[tp, m] = total
-
-    def send_square(k):
-        return pltpu.make_async_remote_copy(
-            src_ref=squares.at[tp], dst_ref=squares.at[tp], send_sem=norm_s.at[k], recv_sem=norm_r.at[k],
-            device_id=(me, (tp + k) % tps), device_id_type=MESH,
-        )
-
-    def recv_square(k):
-        ref = squares.at[(tp + tps - k) % tps]
-        return pltpu.make_async_remote_copy(
-            src_ref=ref, dst_ref=ref, send_sem=norm_s.at[k], recv_sem=norm_r.at[k],
-            device_id=(me, tp), device_id_type=MESH,
-        )
-
-    for k in range(1, tps):
-        send_square(k).start()
-    for m in range(2):
-        update[m] = full_of(m, me)
-    for k in range(1, tps):
-        recv_square(k).wait_recv()
-    copy_gather = Gather(place, 2, lambda block, c: copies.at[c, block], (c_upS, c_upR, c_dnS, c_dnR, c_yS, c_yR))
-    for m in range(2):
-        mean = jnp.sum(jnp.sum(squares[:, m], axis=0), keepdims=True) / entries
+        squares[m, tp] = total
+        for k in range(1, tps):
+            send_square(m, k).start()
+        update[m] = full_of(me)
+
+    copy_gather = Gather(place, 2, lambda block, c: copies.at[c, block], gather_refs[8:])
+    for m in range(2):
+        for k in range(1, tps):
+            recv_square(m, k).wait_recv()
+        mean = jnp.sum(jnp.sum(squares[m], axis=0), keepdims=True) / entries
         new_update = update[m] / jnp.sqrt(mean + 1e-06)
         update[m] = new_update
         new_weight = weights[m] - 0.02 * new_update
@@ -356,25 +463,30 @@
     copy_gather.relay()
 
     gather.finish()
-    small_gather.finish()
     copy_gather.finish()
     for k in range(1, n):
-        hand((me + k) % n).wait_send()
-        send_term(k).wait_send()
-    for k in range(1, tps):
-        send_square(k).wait_send()
+        for c in range(2):
+            hand(side, (me + k) % n, c).wait_send()
+    for m in range(2):
+        for k in range(depth):
+            zi = (z + k) % depth
+            term_cross(m, zi).wait_send()
+            small_cross(m, zi, y).wait_send()
+            if k:
+                term_along(m, zi).wait_send()
+                small_along(m, zi).wait_send()
+        for k in range(1, tps):
+            send_square(m, k).wait_send()
 
 
 def write_kernel(update, fresh, copies, first_new, second_new, *refs):
     outs, sem = refs[:-1], refs[-1]
-    count = 0
     started = []
     for i, source in enumerate((update, fresh, copies, first_new, second_new)):
         for m in range(2):
-            copy = pltpu.make_async_copy(source.at[m], outs[2 * i + m], sem.at[count])
+            copy = pltpu.make_async_copy(source.at[m], outs[2 * i + m], sem.at[2 * i + m])
             copy.start()
             started.append(copy)
-            count += 1
     for copy in started:
         copy.wait()
 
@@ -389,6 +501,7 @@
     dma = pltpu.SemaphoreType.DMA
     vmem = pl.BlockSpec(memory_space=pltpu.VMEM)
     anywhere = pl.BlockSpec(memory_space=pl.ANY)
+    far = pl.BlockSpec(memory_space=pltpu.HBM)
     shape = jax.ShapeDtypeStruct
     results = pl.pallas_call(
         functools.partial(kernel, n, tps, entries),
@@ -397,7 +510,7 @@
             shape((2, n, rows, columns), BF16),
             shape((2, slim, columns), F32), shape((2, slim, columns), F32),
         ),
-        in_specs=[anywhere] * 11,
+        in_specs=[far] * 11,
         out_specs=[vmem] * 5,
         scratch_shapes=[
             pltpu.VMEM((tokens, wide), BF16),
@@ -407,17 +520,20 @@
             pltpu.VMEM((2, slim, columns), F32),
             pltpu.VMEM((2, slim, columns), F32),
             pltpu.VMEM((2, tokens, rank), F32),
-            pltpu.VMEM((n, 2 * slim, columns), F32),
-            pltpu.VMEM((n, 2 * slim, columns), F32),
-            pltpu.VMEM((n, 2 * slim, columns), F32),
-            pltpu.VMEM((tps, 2, 8, columns), F32),
+            pltpu.VMEM((2, n, slim, columns), F32),
+            pltpu.VMEM((2, depth, slim, columns), F32),
+            pltpu.VMEM((2, depth, slim, columns), F32),
+            pltpu.VMEM((2, depth, slim, columns), F32),
+            pltpu.VMEM((2, n, slim, columns), F32),
+            pltpu.VMEM((2, tps, 8, columns), F32),
             dma((11,)),
-            *gather_sems(depth, 1), dma((n,)), dma((n,)), dma((n,)), dma((n,)),
-            *gather_sems(depth, 1), dma((tps,)), dma((tps,)),
-            *gather_sems(depth, 2),
+            dma((n, 2)), dma((n, 2)),
+            *[dma((2, depth))] * 8,
+            dma((2, tps)), dma((2, tps)),
+            *gather_sems(depth, 2), *gather_sems(depth, 2),
         ],
-        compiler_params=pltpu.CompilerParams(collective_id=0, has_side_effects=True, vmem_limit_bytes=48 * 2**20),
-    )(saved_input, cot_inproj, cot_outproj, factor_inproj, *others)
+        compiler_params=pltpu.CompilerParams(collective_id=0, has_side_effects=True, vmem_limit_bytes=40 * 2**20),
+    )(*[pltpu.with_memory_space_constraint(x, pltpu.HBM) for x in (saved_input, cot_inproj, cot_outproj, factor_inproj, *others)])
     update, fresh, copies, first_new, second_new = results
     copies = copies.reshape(2, n * rows, columns)
     return pl.pallas_call(
@@ -425,9 +541,10 @@
         out_shape=(
             *[shape((rows, columns), F32)] * 4, *[shape((n * rows, columns), BF16)] * 2, *[shape((slim, columns), F32)] * 4,
         ),
-        in_specs=[vmem] * 5,
-        out_specs=[anywhere] * 10,
+        in_specs=[anywhere] * 5,
+        out_specs=[far] * 10,
         scratch_shapes=[dma((10,))],
+        compiler_params=pltpu.CompilerParams(vmem_limit_bytes=2**20),
     )(update, fresh, copies, first_new, second_new)
 
 

time: 97.8 us -> 74.2 us (0.76)
  local copies, waits for them, and re-layouts: 12.9 us -> 0 us
  Pallas kernels: 83.6 us -> 73.4 us
    unnamed x30 -> x0, local copies, waits for them, and re-layouts: 12.9 us -> none
    pallas_call x1, Pallas kernels: 79.9 us -> 71.6 us  [kernel_form(): pl.pallas_call(functools.partial(kernel, n, tps, entries), out_shape=(sha...]
    pallas_call x1, Pallas kernels: 3.71 us -> 1.77 us  [kernel_form(): pl.pallas_call(write_kernel, out_shape=(*[shape((rows, columns), F32)] *...]
where the time goes in v2:
time: 74.2 us; the launch traced here: 74 us
  Pallas kernels  73.4 us (99%)
    pallas_call x1, Pallas kernels, kernel_form(): pl.pallas_call(functools.partial(kernel, n, tps, entries), out_shape=(sha...  71.6 us
    pallas_call x1, Pallas kernels, kernel_form(): pl.pallas_call(write_kernel, out_shape=(*[shape((rows, columns), F32)] *...  1.77 us

profile of v2, /device:TPU:0, one launch (start us, length us, event | category | flops | bytes accessed | tf_op | source)
XLA Modules:
  0.0 74.0 jit_solution(5885731274376325949)
XLA Ops:
  0.6 71.6 %shard_map.186 = (f32[2,256,256]{2,1,0:T(8,128)S(1)}, f32[2,256,256]{2,1,0:T(8,128)S(1)}, bf16[2,8,256,256]{3,2,1,0:T(8,128)(2,1)S(1)}, f32[2,32,256]{2,1,0:T(8,128)S(1)}, f32[2,32,256]{2,1,0:T(8,128)S(1)}) custom-call(bf16[768,2048]{1,0:T(8,128)(2,1)} %saved_hbm.1, bf16[768,256]{1,0:T(8,128)(2,1)} %cot_in_hbm.1, bf16[768,256]{1,0:T(8,128)(2,1)} %cot_out_hbm.1, ...), custom_call_target="tpu_custom_call" | custom-call | tf_op jit(solution)/shard_map/pallas_call | solution.py:506
  72.2 1.8 %shard_map.187 = (f32[256,256]{1,0:T(8,128)}, f32[256,256]{1,0:T(8,128)}, f32[256,256]{1,0:T(8,128)}, f32[256,256]{1,0:T(8,128)}, bf16[2048,256]{1,0:T(8,128)(2,...) custom-call(f32[2,256,256]{2,1,0:T(8,128)S(1)} %get-tuple-element.15, ...), custom_call_target="tpu_custom_call" | custom-call | tf_op jit(solution)/shard_map/pallas_call | solution.py:539

commit v3 on v2

--- a/solution.py
+++ b/solution.py
@@ -100,8 +100,23 @@
 
 
 class Gather:
-    def __init__(self, place, chunks, ref_of, sems):
+    def goes_up(self, s):
+        z, last = self.z, self.depth - 1
+        needed = (z - s >= 0) & (z < last)
+        return needed & (z != last - 1) if self.near and s == 0 else needed
+
+    def goes_down(self, s):
+        z, last = self.z, self.depth - 1
+        needed = (z + s <= last) & (z >= 1)
+        return needed & (z != 1) if self.near and s == 0 else needed
+
+    def crosses(self, zi, c):
+        sent = jnp.logical_not(self.detour(zi, c))
+        return sent & (zi != self.z) if self.near else sent
+
+    def __init__(self, place, chunks, ref_of, sems, near=False):
         self.z, self.y, self.tp, self.depth = place
+        self.near = near
         self.chunks, self.ref_of = chunks, ref_of
         self.up_s, self.up_r, self.dn_s, self.dn_r, self.y_s, self.y_r, self.x_s, self.x_r = sems
 
@@ -110,7 +125,7 @@
         if self.depth < 4:
             return z < 0
         end = ((z == 1) & (zi == 0)) | ((z == last - 1) & (zi == last))
-        if c == self.chunks - 1:
+        if c >= self.chunks // 2:
             end = end | ((z == 0) & (zi == 1)) | ((z == last) & (zi == last - 1))
         return end
 
@@ -150,20 +165,27 @@
             return ()
         z, last = self.z, self.depth - 1
         cases = [(z == 0, 1), (z == last, last - 1)]
-        if c == self.chunks - 1:
+        if c >= self.chunks // 2:
             cases += [(z == 1, 0), (z == last - 1, last)]
         return cases
 
     def start(self, c):
-        @pl.when(self.z + 1 < self.depth)
+        @pl.when(self.goes_up(0))
         def _():
             self.up(0, c).start()
 
-        @pl.when(self.z >= 1)
+        @pl.when(self.goes_down(0))
         def _():
             self.down(0, c).start()
 
-        self.across(self.z, c).start()
+        if not self.near:
+            self.across(self.z, c).start()
+
+    def start_beside(self, c):
+        for condition, neighbour in self.beside_cases(c):
+            @pl.when(condition)
+            def _():
+                self.beside(c, neighbour).start()
 
     def hand_on(self, zi, c):
         @pl.when(jnp.logical_not(self.detour(zi, c)))
@@ -191,7 +213,12 @@
                 if s < depth:
                     @pl.when(z - s >= 0)
                     def _():
-                        self.from_below(s - 1, c).wait_recv()
+                        if self.near and s == 1:
+                            @pl.when(z != depth - 1)
+                            def _():
+                                self.from_below(0, c).wait_recv()
+                        else:
+                            self.from_below(s - 1, c).wait_recv()
                         if s < depth - 1:
                             @pl.when(z + 1 < depth)
                             def _():
@@ -201,7 +228,12 @@
 
                     @pl.when(z + s < depth)
                     def _():
-                        self.from_above(s - 1, c).wait_recv()
+                        if self.near and s == 1:
+                            @pl.when(z != 0)
+                            def _():
+                                self.from_above(0, c).wait_recv()
+                        else:
+                            self.from_above(s - 1, c).wait_recv()
                         if s < depth - 1:
                             @pl.when(z >= 1)
                             def _():
@@ -210,12 +242,10 @@
                         have((z + s) * 2 + self.y, c)
 
                 if s == 1:
-                    self.from_across(z, c).wait_recv()
-                    for condition, neighbour in self.beside_cases(c):
-                        @pl.when(condition)
-                        def _():
-                            self.beside(c, neighbour).start()
-                    have(z * 2 + 1 - self.y, c)
+                    if not self.near:
+                        self.from_across(z, c).wait_recv()
+                        self.start_beside(c)
+                        have(z * 2 + 1 - self.y, c)
                 else:
                     @pl.when(z - (s - 1) >= 0)
                     def _():
@@ -230,15 +260,15 @@
     def finish(self):
         for c in range(self.chunks):
             for s in range(self.depth - 1):
-                @pl.when((self.z - s >= 0) & (self.z + 1 < self.depth))
+                @pl.when(self.goes_up(s))
                 def _():
                     self.up(s, c).wait_send()
 
-                @pl.when((self.z + s < self.depth) & (self.z >= 1))
+                @pl.when(self.goes_down(s))
                 def _():
                     self.down(s, c).wait_send()
             for zi in range(self.depth):
-                @pl.when(jnp.logical_not(self.detour(zi, c)))
+                @pl.when(self.crosses(zi, c))
                 def _():
                     self.across(zi, c).wait_send()
             for condition, neighbour in self.beside_cases(c):
@@ -257,8 +287,8 @@
     saved_hbm, cot_in_hbm, cot_out_hbm, factor_in_hbm, factor_out_hbm, weight_in_hbm, weight_out_hbm,
     first_in_hbm, first_out_hbm, second_in_hbm, second_out_hbm,
     update, fresh, copies, first_new, second_new,
-    saved, cots, factors, weights, first, second, mapped, terms, crossed, staged, landed, smalls, squares,
-    load_sem, pair_s, pair_r, ty_s, ty_r, tz_s, tz_r, sz_s, sz_r, sy_s, sy_r, norm_s, norm_r, *gather_refs,
+    saved, cots, factors, weights, first, second, mapped, terms, crossed, staged, landed, smalls, squares, early, ahead,
+    wy_s, wy_r, wz_s, wz_r, load_sem, pair_s, pair_r, ty_s, ty_r, tz_s, tz_r, sz_s, sz_r, sy_s, sy_r, norm_s, norm_r, *gather_refs,
 ):
     me, tp = lax.axis_index("fs"), lax.axis_index("tp")
     z, y = me // 2, me % 2
@@ -334,11 +364,38 @@
             map_handed((z + distance) * 2 + y)
             map_handed((z + distance) * 2 + 1 - y)
 
+    at_end = (z == 0) | (z == depth - 1)
+    inner = jnp.where(z == 0, 1, depth - 2)
+    by_end = (z == 1) | (z == depth - 2)
+    outer = jnp.where(z == 1, 0, depth - 1)
+
+    def early_cross(m, c):
+        return pltpu.make_async_remote_copy(
+            src_ref=weights.at[m, pl.ds(c * half, half)], dst_ref=early.at[0, m, pl.ds(c * half, half)],
+            send_sem=wy_s.at[m, c], recv_sem=wy_r.at[m, c], device_id=(z * 2 + 1 - y, tp), device_id_type=MESH,
+        )
+
+    def early_along(m, c):
+        return pltpu.make_async_remote_copy(
+            src_ref=weights.at[m, pl.ds(c * half, half)], dst_ref=early.at[1, m, pl.ds(c * half, half)],
+            send_sem=wz_s.at[m, c], recv_sem=wz_r.at[m, c], device_id=(outer * 2 + y, tp), device_id_type=MESH,
+        )
+
+    def early_along_start(m):
+        @pl.when(by_end)
+        def _():
+            for c in range(2):
+                early_along(m, c).start()
+
     map_block(me, True)
     gather.relay(
         lambda block, c: hand(side, block, c).start(),
         lambda s: map_at(s - 2) if s >= 2 else None,
     )
+    for load in loads[3:]:
+        load.wait()
+    early_cross(0, 0).start()
+    early_along_start(0)
     map_at(depth - 1)
 
     def term_cross(m, zi):
@@ -361,8 +418,6 @@
         )
 
     order = [k % depth for k in range(1, depth + 1)]
-    for load in loads[3:]:
-        load.wait()
     for m in range(2):
         high, middle, low = parts_of(mapped[m].T)
         term = dot(high, cots[m]) + (dot(middle, cots[m]) + dot(low, cots[m]))
@@ -376,6 +431,8 @@
             staged[m, zi] = terms[m, zi * 2 + y] + crossed[m, zi]
             if k:
                 term_along(m, zi).start()
+
+    early_cross(0, 1).start()
 
     def small_along(m, zi):
         ref = smalls.at[m, me]
@@ -430,6 +487,16 @@
             device_id=(me, tp), device_id_type=MESH,
         )
 
+    early_cross(1, 0).start()
+    early_cross(1, 1).start()
+    early_along_start(1)
+
+    def chunk_ref(block, c):
+        return copies.at[c // 2, block, pl.ds(c % 2 * half, half)]
+
+    copy_gather = Gather(place, 4, chunk_ref, gather_refs[8:], near=True)
+    beside = z * 2 + 1 - y
+    behind = inner * 2 + y
     for m in range(2):
         for k in range(depth):
             small_cross(m, (z + k) % depth, 1 - y).wait_recv()
@@ -448,20 +515,44 @@
         for k in range(1, tps):
             send_square(m, k).start()
         update[m] = full_of(me)
-
-    copy_gather = Gather(place, 2, lambda block, c: copies.at[c, block], gather_refs[8:])
-    for m in range(2):
+        ahead[0] = full_of(beside)
+
+        @pl.when(at_end)
+        def _():
+            ahead[1] = full_of(behind)
+
         for k in range(1, tps):
             recv_square(m, k).wait_recv()
         mean = jnp.sum(jnp.sum(squares[m], axis=0), keepdims=True) / entries
-        new_update = update[m] / jnp.sqrt(mean + 1e-06)
+        root = jnp.sqrt(mean + 1e-06)
+        new_update = update[m] / root
+        new_weight = weights[m] - 0.02 * new_update
+        copies[m, me] = new_weight.astype(BF16)
+        for c in range(2 * m, 2 * m + 2):
+            copy_gather.start(c)
         update[m] = new_update
-        new_weight = weights[m] - 0.02 * new_update
         fresh[m] = new_weight
-        copies[m, me] = new_weight.astype(BF16)
-        copy_gather.start(m)
+        for c in range(2):
+            early_cross(m, c).wait_recv()
+        copies[m, beside] = (early[0, m] - 0.02 * (ahead[0] / root)).astype(BF16)
+        for c in range(2 * m, 2 * m + 2):
+            copy_gather.start_beside(c)
+
+        @pl.when(at_end)
+        def _():
+            for c in range(2):
+                early_along(m, c).wait_recv()
+            copies[m, behind] = (early[1, m] - 0.02 * (ahead[1] / root)).astype(BF16)
+
     copy_gather.relay()
 
+    for m in range(2):
+        for c in range(2):
+            early_cross(m, c).wait_send()
+
+            @pl.when(by_end)
+            def _():
+                early_along(m, c).wait_send()
     gather.finish()
     copy_gather.finish()
     for k in range(1, n):
@@ -526,11 +617,14 @@
             pltpu.VMEM((2, depth, slim, columns), F32),
             pltpu.VMEM((2, n, slim, columns), F32),
             pltpu.VMEM((2, tps, 8, columns), F32),
+            pltpu.VMEM((2, 2, rows, columns), F32),
+            pltpu.VMEM((2, rows, columns), F32),
+            *[dma((2, 2))] * 4,
             dma((11,)),
             dma((n, 2)), dma((n, 2)),
             *[dma((2, depth))] * 8,
             dma((2, tps)), dma((2, tps)),
-            *gather_sems(depth, 2), *gather_sems(depth, 2),
+            *gather_sems(depth, 2), *gather_sems(depth, 4),
         ],
         compiler_params=pltpu.CompilerParams(collective_id=0, has_side_effects=True, vmem_limit_bytes=40 * 2**20),
     )(*[pltpu.with_memory_space_constraint(x, pltpu.HBM) for x in (saved_input, cot_inproj, cot_outproj, factor_inproj, *others)])
@@ -551,7 +645,7 @@
 def on_device(saved_input, cot_inproj, cot_outproj, factor_inproj, *others):
     n, tps = lax.axis_size("fs"), lax.axis_size("tp")
     rows, rank = factor_inproj.shape
-    if n % 2 == 0 and n >= 4 and tps % 2 == 0 and rank % (8 * n) == 0 and rows % 128 == 0 and cot_inproj.shape[1] % 128 == 0:
+    if n % 2 == 0 and n >= 8 and tps % 2 == 0 and rank % (8 * n) == 0 and rows % 128 == 0 and cot_inproj.shape[1] % 128 == 0:
         return kernel_form(n, tps, saved_input, cot_inproj, cot_outproj, factor_inproj, *others)
     return plain_form(saved_input, cot_inproj, cot_outproj, factor_inproj, *others)
 

time: 74.2 us -> 73.3 us (0.988)
  Pallas kernels: 73.4 us -> 72.5 us
    pallas_call x1, Pallas kernels: 71.6 us -> 70.7 us  [kernel_form(): pl.pallas_call(functools.partial(kernel, n, tps, entries), out_shape=(sha...]
where the time goes in v3:
time: 73.3 us; the launch traced here: 73.2 us
  Pallas kernels  72.5 us (99%)
    pallas_call x1, Pallas kernels, kernel_form(): pl.pallas_call(functools.partial(kernel, n, tps, entries), out_shape=(sha...  70.7 us
    pallas_call x1, Pallas kernels, kernel_form(): pl.pallas_call(write_kernel, out_shape=(*[shape((rows, columns), F32)] *...  1.77 us

profile of v3, /device:TPU:0, one launch (start us, length us, event | category | flops | bytes accessed | tf_op | source)
XLA Modules:
  0.0 73.2 jit_solution(17230720002343391033)
XLA Ops:
  0.6 70.7 %shard_map.186 = (f32[2,256,256]{2,1,0:T(8,128)S(1)}, f32[2,256,256]{2,1,0:T(8,128)S(1)}, bf16[2,8,256,256]{3,2,1,0:T(8,128)(2,1)S(1)}, f32[2,32,256]{2,1,0:T(8,128)S(1)}, f32[2,32,256]{2,1,0:T(8,128)S(1)}) custom-call(bf16[768,2048]{1,0:T(8,128)(2,1)} %saved_hbm.1, bf16[768,256]{1,0:T(8,128)(2,1)} %cot_in_hbm.1, bf16[768,256]{1,0:T(8,128)(2,1)} %cot_out_hbm.1, ...), custom_call_target="tpu_custom_call" | custom-call | tf_op jit(solution)/shard_map/pallas_call | solution.py:597
  71.4 1.8 %shard_map.187 = (f32[256,256]{1,0:T(8,128)}, f32[256,256]{1,0:T(8,128)}, f32[256,256]{1,0:T(8,128)}, f32[256,256]{1,0:T(8,128)}, bf16[2048,256]{1,0:T(8,128)(2,...) custom-call(f32[2,256,256]{2,1,0:T(8,128)S(1)} %get-tuple-element.15, ...), custom_call_target="tpu_custom_call" | custom-call | tf_op jit(solution)/shard_map/pallas_call | solution.py:633

commit v4 on v3

--- a/solution.py
+++ b/solution.py
@@ -288,7 +288,7 @@
     first_in_hbm, first_out_hbm, second_in_hbm, second_out_hbm,
     update, fresh, copies, first_new, second_new,
     saved, cots, factors, weights, first, second, mapped, terms, crossed, staged, landed, smalls, squares, early, ahead,
-    wy_s, wy_r, wz_s, wz_r, load_sem, pair_s, pair_r, ty_s, ty_r, tz_s, tz_r, sz_s, sz_r, sy_s, sy_r, norm_s, norm_r, *gather_refs,
+    wy_s, wy_r, wz_s, wz_r, twin_s, twin_r, load_sem, pair_s, pair_r, ty_s, ty_r, tz_s, tz_r, sz_s, sz_r, sy_s, sy_r, norm_s, norm_r, *gather_refs,
 ):
     me, tp = lax.axis_index("fs"), lax.axis_index("tp")
     z, y = me // 2, me % 2
@@ -323,17 +323,33 @@
     loads[1].wait()
     pl.semaphore_wait(barrier, depth + tps - 1)
 
-    def factor_ref(m, block, c):
-        return factors.at[m, block, pl.ds(c * half, half)]
-
-    def hand(m, block, c):
-        ref = factor_ref(m, block, c)
-        return pltpu.make_async_remote_copy(
-            src_ref=ref, dst_ref=ref, send_sem=pair_s.at[block, c], recv_sem=pair_r.at[block, c],
+    quarter = half // 2
+    group = tp // 2
+    twin = (tp + 2) % tps
+
+    def factor_ref(m, block, h, c):
+        return factors.at[m, block, pl.ds(pl.multiple_of(h * half + c * quarter, quarter), quarter)]
+
+    def hand(m, block, h, c):
+        ref = factor_ref(m, block, h, c)
+        at = h * 2 + c
+        return pltpu.make_async_remote_copy(
+            src_ref=ref, dst_ref=ref, send_sem=pair_s.at[block, at], recv_sem=pair_r.at[block, at],
             device_id=(me, partner), device_id_type=MESH,
         )
 
-    gather = Gather(place, 2, lambda block, c: factor_ref(side, block, c), gather_refs[:8])
+    def share(block, h, c):
+        ref = factor_ref(side, block, h, c)
+        return pltpu.make_async_remote_copy(
+            src_ref=ref, dst_ref=ref, send_sem=twin_s.at[block, c], recv_sem=twin_r.at[block, c],
+            device_id=(me, twin), device_id_type=MESH,
+        )
+
+    def have_factor(block, c):
+        share(block, group, c).start()
+        hand(side, block, group, c).start()
+
+    gather = Gather(place, 2, lambda block, c: factor_ref(side, block, group, c), gather_refs[:8])
     gather.start(0)
     gather.start(1)
     loads[2].wait()
@@ -344,10 +360,16 @@
             product = dot(piece, factors[m, block])
             mapped[m] = product if first_one else mapped[m] + product
 
-    def map_handed(block):
-        for c in range(2):
-            hand(1 - side, block, c).wait_recv()
-        map_block(block)
+    def map_handed(*blocks):
+        for block in blocks:
+            for c in range(2):
+                share(block, 1 - group, c).wait_recv()
+                hand(side, block, 1 - group, c).start()
+        for block in blocks:
+            for h in range(2):
+                for c in range(2):
+                    hand(1 - side, block, h, c).wait_recv()
+            map_block(block)
 
     def map_at(distance):
         if distance == 0:
@@ -356,13 +378,11 @@
 
         @pl.when(z - distance >= 0)
         def _():
-            map_handed((z - distance) * 2 + y)
-            map_handed((z - distance) * 2 + 1 - y)
+            map_handed((z - distance) * 2 + y, (z - distance) * 2 + 1 - y)
 
         @pl.when(z + distance < depth)
         def _():
-            map_handed((z + distance) * 2 + y)
-            map_handed((z + distance) * 2 + 1 - y)
+            map_handed((z + distance) * 2 + y, (z + distance) * 2 + 1 - y)
 
     at_end = (z == 0) | (z == depth - 1)
     inner = jnp.where(z == 0, 1, depth - 2)
@@ -388,14 +408,18 @@
                 early_along(m, c).start()
 
     map_block(me, True)
-    gather.relay(
-        lambda block, c: hand(side, block, c).start(),
-        lambda s: map_at(s - 2) if s >= 2 else None,
-    )
     for load in loads[3:]:
         load.wait()
-    early_cross(0, 0).start()
-    early_along_start(0)
+
+    def after_step(s):
+        if s == depth - 1:
+            early_cross(0, 0).start()
+            early_cross(0, 1).start()
+            early_along_start(0)
+        if s >= 2:
+            map_at(s - 2)
+
+    gather.relay(have_factor, after_step)
     map_at(depth - 1)
 
     def term_cross(m, zi):
@@ -431,8 +455,6 @@
             staged[m, zi] = terms[m, zi * 2 + y] + crossed[m, zi]
             if k:
                 term_along(m, zi).start()
-
-    early_cross(0, 1).start()
 
     def small_along(m, zi):
         ref = smalls.at[m, me]
@@ -557,7 +579,9 @@
     copy_gather.finish()
     for k in range(1, n):
         for c in range(2):
-            hand(side, (me + k) % n, c).wait_send()
+            share((me + k) % n, group, c).wait_send()
+            for h in range(2):
+                hand(side, (me + k) % n, h, c).wait_send()
     for m in range(2):
         for k in range(depth):
             zi = (z + k) % depth
@@ -620,8 +644,9 @@
             pltpu.VMEM((2, 2, rows, columns), F32),
             pltpu.VMEM((2, rows, columns), F32),
             *[dma((2, 2))] * 4,
+            dma((n, 2)), dma((n, 2)),
             dma((11,)),
-            dma((n, 2)), dma((n, 2)),
+            dma((n, 4)), dma((n, 4)),
             *[dma((2, depth))] * 8,
             dma((2, tps)), dma((2, tps)),
             *gather_sems(depth, 2), *gather_sems(depth, 4),
@@ -645,7 +670,7 @@
 def on_device(saved_input, cot_inproj, cot_outproj, factor_inproj, *others):
     n, tps = lax.axis_size("fs"), lax.axis_size("tp")
     rows, rank = factor_inproj.shape
-    if n % 2 == 0 and n >= 8 and tps % 2 == 0 and rank % (8 * n) == 0 and rows % 128 == 0 and cot_inproj.shape[1] % 128 == 0:
+    if n % 2 == 0 and n >= 8 and tps == 4 and rank % (8 * n) == 0 and rows % 128 == 0 and cot_inproj.shape[1] % 128 == 0:
         return kernel_form(n, tps, saved_input, cot_inproj, cot_outproj, factor_inproj, *others)
     return plain_form(saved_input, cot_inproj, cot_outproj, factor_inproj, *others)
 

time: 73.3 us -> 75.4 us (1.029)
  Pallas kernels: 72.5 us -> 74.6 us
    pallas_call x1, Pallas kernels: 70.7 us -> 72.8 us  [kernel_form(): pl.pallas_call(functools.partial(kernel, n, tps, entries), out_shape=(sha...]
where the time goes in v4:
time: 75.4 us; the launch traced here: 75.2 us
  Pallas kernels  74.6 us (99%)
    pallas_call x1, Pallas kernels, kernel_form(): pl.pallas_call(functools.partial(kernel, n, tps, entries), out_shape=(sha...  72.8 us
    pallas_call x1, Pallas kernels, kernel_form(): pl.pallas_call(write_kernel, out_shape=(*[shape((rows, columns), F32)] *...  1.77 us

profile of v4, /device:TPU:0, one launch (start us, length us, event | category | flops | bytes accessed | tf_op | source)
XLA Modules:
  0.0 75.2 jit_solution(4419056554030569200)
XLA Ops:
  0.6 72.8 %shard_map.186 = (f32[2,256,256]{2,1,0:T(8,128)S(1)}, f32[2,256,256]{2,1,0:T(8,128)S(1)}, bf16[2,8,256,256]{3,2,1,0:T(8,128)(2,1)S(1)}, f32[2,32,256]{2,1,0:T(8,128)S(1)}, f32[2,32,256]{2,1,0:T(8,128)S(1)}) custom-call(bf16[768,2048]{1,0:T(8,128)(2,1)} %saved_hbm.1, bf16[768,256]{1,0:T(8,128)(2,1)} %cot_in_hbm.1, bf16[768,256]{1,0:T(8,128)(2,1)} %cot_out_hbm.1, ...), custom_call_target="tpu_custom_call" | custom-call | tf_op jit(solution)/shard_map/pallas_call | solution.py:621
  73.5 1.8 %shard_map.187 = (f32[256,256]{1,0:T(8,128)}, f32[256,256]{1,0:T(8,128)}, f32[256,256]{1,0:T(8,128)}, f32[256,256]{1,0:T(8,128)}, bf16[2048,256]{1,0:T(8,128)(2,...) custom-call(f32[2,256,256]{2,1,0:T(8,128)S(1)} %get-tuple-element.15, ...), custom_call_target="tpu_custom_call" | custom-call | tf_op jit(solution)/shard_map/pallas_call | solution.py:658

commit v5 on v3

--- a/solution.py
+++ b/solution.py
@@ -297,6 +297,7 @@
     partner = tp + 1 - 2 * side
     rows = factors.shape[2]
     half = rows // 2
+    quarter = rows // 4
     slim = first.shape[1]
     place = (z, y, tp, depth)
 
@@ -324,7 +325,7 @@
     pl.semaphore_wait(barrier, depth + tps - 1)
 
     def factor_ref(m, block, c):
-        return factors.at[m, block, pl.ds(c * half, half)]
+        return factors.at[m, block, pl.ds(c * quarter, quarter)]
 
     def hand(m, block, c):
         ref = factor_ref(m, block, c)
@@ -333,9 +334,9 @@
             device_id=(me, partner), device_id_type=MESH,
         )
 
-    gather = Gather(place, 2, lambda block, c: factor_ref(side, block, c), gather_refs[:8])
-    gather.start(0)
-    gather.start(1)
+    gather = Gather(place, 4, lambda block, c: factor_ref(side, block, c), gather_refs[:8])
+    for c in range(4):
+        gather.start(c)
     loads[2].wait()
 
     def map_block(block, first_one=False):
@@ -345,7 +346,7 @@
             mapped[m] = product if first_one else mapped[m] + product
 
     def map_handed(block):
-        for c in range(2):
+        for c in range(4):
             hand(1 - side, block, c).wait_recv()
         map_block(block)
 
@@ -556,7 +557,7 @@
     gather.finish()
     copy_gather.finish()
     for k in range(1, n):
-        for c in range(2):
+        for c in range(4):
             hand(side, (me + k) % n, c).wait_send()
     for m in range(2):
         for k in range(depth):
@@ -621,10 +622,10 @@
             pltpu.VMEM((2, rows, columns), F32),
             *[dma((2, 2))] * 4,
             dma((11,)),
-            dma((n, 2)), dma((n, 2)),
+            dma((n, 4)), dma((n, 4)),
             *[dma((2, depth))] * 8,
             dma((2, tps)), dma((2, tps)),
-            *gather_sems(depth, 2), *gather_sems(depth, 4),
+            *gather_sems(depth, 4), *gather_sems(depth, 4),
         ],
         compiler_params=pltpu.CompilerParams(collective_id=0, has_side_effects=True, vmem_limit_bytes=40 * 2**20),
     )(*[pltpu.with_memory_space_constraint(x, pltpu.HBM) for x in (saved_input, cot_inproj, cot_outproj, factor_inproj, *others)])

time: 73.3 us -> 73.7 us (level)
  no operation moved by 1% of the time
where the time goes in v5:
time: 73.7 us; the launch traced here: 73.6 us
  Pallas kernels  72.9 us (99%)
    pallas_call x1, Pallas kernels, kernel_form(): pl.pallas_call(functools.partial(kernel, n, tps, entries), out_shape=(sha...  71.2 us
    pallas_call x1, Pallas kernels, kernel_form(): pl.pallas_call(write_kernel, out_shape=(*[shape((rows, columns), F32)] *...  1.77 us

profile of v5, /device:TPU:0, one launch (start us, length us, event | category | flops | bytes accessed | tf_op | source)
XLA Modules:
  0.0 73.6 jit_solution(8912860288014374115)
XLA Ops:
  0.6 71.2 %shard_map.186 = (f32[2,256,256]{2,1,0:T(8,128)S(1)}, f32[2,256,256]{2,1,0:T(8,128)S(1)}, bf16[2,8,256,256]{3,2,1,0:T(8,128)(2,1)S(1)}, f32[2,32,256]{2,1,0:T(8,128)S(1)}, f32[2,32,256]{2,1,0:T(8,128)S(1)}) custom-call(bf16[768,2048]{1,0:T(8,128)(2,1)} %saved_hbm.1, bf16[768,256]{1,0:T(8,128)(2,1)} %cot_in_hbm.1, bf16[768,256]{1,0:T(8,128)(2,1)} %cot_out_hbm.1, ...), custom_call_target="tpu_custom_call" | custom-call | tf_op jit(solution)/shard_map/pallas_call | solution.py:598
  71.8 1.8 %shard_map.187 = (f32[256,256]{1,0:T(8,128)}, f32[256,256]{1,0:T(8,128)}, f32[256,256]{1,0:T(8,128)}, f32[256,256]{1,0:T(8,128)}, bf16[2048,256]{1,0:T(8,128)(2,...) custom-call(f32[2,256,256]{2,1,0:T(8,128)S(1)} %get-tuple-element.15, ...), custom_call_target="tpu_custom_call" | custom-call | tf_op jit(solution)/shard_map/pallas_call | solution.py:634
